TPU v7x, 256 devices: a 4x2x16 block of a 4x16x16 slice. The times are simulated.
256 devices in a mesh: grp: 2 (over y), sp: 32 (over z, core), tp: 4 (over x).
Axes of the slice: x: 4, y: 2, z: 16, core: 2. Of those that a mesh axis runs over, the one named last changes fastest.
The devices are a block of a 4x16x16 slice.
Arguments:
- query_nope: bfloat16 [20480, 1024], P(('grp', 'sp'), 'tp'), parts along dimension 0, may hold values from -12 to 12
- query_rope: bfloat16 [20480, 512], P(('grp', 'sp'), 'tp'), parts along dimension 0, may hold values from -48 to 48
- token_latent: bfloat16 [20480, 256], P(('grp', 'sp')), parts along dimension 0, may hold values from -6 to 6
- key_rope: bfloat16 [20480, 32], P(('grp', 'sp')), parts along dimension 0, may hold values from -48 to 48
- latent_norm_gain: float32 [256], replicated, may hold values from 0.1 to 1.9
- key_expand_weight: bfloat16 [256, 1024], replicated, may hold values from -0.375 to 0.375
- value_expand_weight: bfloat16 [256, 1024], replicated, may hold values from -0.375 to 0.375
- residual: bfloat16 [20480, 2048], P(('grp', 'sp')), parts along dimension 0, may hold values from -3 to 3
- out_weight: bfloat16 [1024, 2048], P('tp'), may hold values from -0.375 to 0.375
- ffn_gain: float32 [2048], replicated, may hold values from 0.1 to 1.9
- gate_weight: bfloat16 [2048, 5632], P('sp', 'tp'), may hold values from -0.125 to 0.125
- up_weight: bfloat16 [2048, 5632], P('sp', 'tp'), may hold values from -0.125 to 0.125
- down_weight: bfloat16 [5632, 2048], P('tp', 'sp'), may hold values from -0.078125 to 0.078125
Outputs:
- layer_output: bfloat16 [20480, 2048], P(('grp', 'sp', 'tp')), parts along dimension 0
There are 2 independent parts, one for each index of `grp`. A program takes and returns all parts, laid end to end along the dimension named above; an argument that names none is the same for every part. Nothing has to cross between parts.
All inputs are finite; a program needn't handle non-finite values.
Results may differ from a plain program's by a relative error of at most 0.015.
Values may be sent and summed in bfloat16 or wider, within the bound.
No kernel may reach another device: no remote copies, remote signals or barrier semaphores. Data moves between devices by JAX's collectives and lax.ppermute only.
A program may use at most 128 MiB of HBM per device.

v0:
```python
import jax
import jax.numpy as jnp
from jax import lax
from jax.sharding import PartitionSpec as P

UNROTATED_SIZE = 64
ROPE = 32
VALUE_SIZE = 64
GRID_W = 64


def side_by_side(arrays, axis, dim, along):
    widths = [a.shape[along] for a in arrays]
    both = jnp.concatenate(arrays, axis=along)
    whole = lax.all_gather(both, axis, axis=dim, tiled=True)
    return tuple(jnp.split(whole, [sum(widths[:k]) for k in range(1, len(widths))], axis=along))


def cut_along(array, dim, count):
    dims = array.shape
    parts = array.reshape(*dims[:dim], count, dims[dim] // count, *dims[dim + 1 :])
    return jnp.moveaxis(parts, dim, 0)


def summed_on_arrival(array, axis, dim):
    count = lax.axis_size(axis)
    parts = lax.all_to_all(cut_along(array, dim, count), axis, 0, 0, tiled=True)
    return jnp.sum(parts.astype(jnp.float32), axis=0)


def sent_to_all(array, axis):
    copies = jnp.broadcast_to(array, (lax.axis_size(axis), *array.shape))
    return lax.all_to_all(copies, axis, split_axis=0, concat_axis=0, tiled=True)


def joined_along(parts, dim):
    dims = list(parts.shape[1:])
    dims[dim] *= parts.shape[0]
    return jnp.moveaxis(parts, 0, dim).reshape(dims)


def collect(array, axis, dim):
    parts = sent_to_all(array, axis)
    return joined_along(parts, dim)


def norm_rows(values, gain):
    wide = values.astype(jnp.float32)
    return wide * lax.rsqrt(jnp.mean(wide * wide, axis=-1, keepdims=True) + 1e-06) * gain


def turn_heads(vectors, positions):
    tokens, heads, width = vectors.shape
    freqs = width // 4
    grid_pos = jnp.stack([positions // GRID_W, positions % GRID_W], axis=-1).astype(jnp.float32)
    inverse = jnp.power(10000.0, -jnp.arange(freqs, dtype=jnp.float32) / freqs)
    angles = grid_pos[:, :, None] * inverse
    cosine = jnp.cos(angles)[:, None]
    sine = jnp.sin(angles)[:, None]
    viewed = vectors.reshape(tokens, heads, 2, 2, freqs)
    first = viewed[..., 0, :]
    second = viewed[..., 1, :]
    turned = jnp.stack([first * cosine - second * sine, first * sine + second * cosine], axis=-2)
    return turned.reshape(tokens, heads, width)


def local(
    query_nope,
    query_rope,
    token_latent,
    key_rope,
    latent_norm_gain,
    key_expand_weight,
    value_expand_weight,
    residual,
    out_weight,
    ffn_gain,
    gate_weight,
    up_weight,
    down_weight,
):
    tok_rows = query_nope.shape[0]
    heads_here = query_nope.shape[1] // UNROTATED_SIZE
    own_rows = tok_rows // lax.axis_size("tp")
    tp_index = lax.axis_index("tp")
    positions = lax.axis_index("sp") * tok_rows + jnp.arange(tok_rows, dtype=jnp.int32)
    gate_full, up_full = side_by_side((gate_weight, up_weight), "sp", 0, 1)
    query_flat = query_nope.reshape(tok_rows, heads_here, UNROTATED_SIZE)
    query_turned = turn_heads(
        query_rope.astype(jnp.float32).reshape(tok_rows, heads_here, ROPE), positions
    ).astype(jnp.bfloat16)
    latent = norm_rows(token_latent, latent_norm_gain).astype(jnp.bfloat16)
    key_turned = turn_heads(key_rope.astype(jnp.float32)[:, None, :], positions)[:, 0].astype(
        jnp.bfloat16
    )
    key_cols = lax.dynamic_slice_in_dim(
        key_expand_weight, tp_index * heads_here * UNROTATED_SIZE, heads_here * UNROTATED_SIZE, 1
    )
    value_cols = lax.dynamic_slice_in_dim(
        value_expand_weight, tp_index * heads_here * VALUE_SIZE, heads_here * VALUE_SIZE, 1
    )
    score_scale = (UNROTATED_SIZE + ROPE) ** (-0.5)

    def absorb(carried, block_in):
        latent_block, rope_block = block_in
        block_rows = latent_block.shape[0]
        key_rows = jnp.dot(latent_block, key_cols, preferred_element_type=jnp.float32).astype(
            jnp.bfloat16
        )
        key_rows = key_rows.reshape(block_rows, heads_here, UNROTATED_SIZE)
        value_rows = jnp.dot(latent_block, value_cols, preferred_element_type=jnp.float32).astype(
            jnp.bfloat16
        )
        value_rows = value_rows.reshape(block_rows, heads_here, VALUE_SIZE)
        scores = (
            jnp.einsum("qhd,khd->hqk", query_flat, key_rows, preferred_element_type=jnp.float32)
            + jnp.einsum(
                "qhd,kd->hqk", query_turned, rope_block, preferred_element_type=jnp.float32
            )
        ) * score_scale
        highest, totals, accumulated = carried
        new_highest = jnp.maximum(highest, jnp.max(scores, axis=-1))
        shrink = jnp.exp(highest - new_highest)
        weights = jnp.exp(scores - new_highest[:, :, None])
        totals = totals * shrink + jnp.sum(weights, axis=-1)
        accumulated = accumulated * shrink.T[:, :, None] + jnp.einsum(
            "hqk,khd->qhd",
            weights.astype(jnp.bfloat16),
            value_rows,
            preferred_element_type=jnp.float32,
        )
        return ((new_highest, totals, accumulated), None)

    initial = (
        jnp.full((heads_here, tok_rows), -jnp.inf, jnp.float32),
        jnp.zeros((heads_here, tok_rows), jnp.float32),
        jnp.zeros((tok_rows, heads_here, VALUE_SIZE), jnp.float32),
    )
    carried = initial
    latent_piece = lax.all_gather(latent, "sp", axis=0, tiled=True)
    rope_piece = lax.all_gather(key_turned, "sp", axis=0, tiled=True)
    shard_count = latent_piece.shape[0] // tok_rows
    grouped = max(
        (
            factor
            for factor in range(1, shard_count + 1)
            if shard_count % factor == 0 and factor * tok_rows <= max(1024, tok_rows)
        )
    )
    block_rows = grouped * tok_rows
    blocks = (
        latent_piece.reshape(-1, block_rows, latent_piece.shape[1]),
        rope_piece.reshape(-1, block_rows, rope_piece.shape[1]),
    )
    carried, _ = lax.scan(absorb, carried, blocks)
    highest, totals, accumulated = carried
    attended = (
        (accumulated / totals.T[:, :, None])
        .reshape(tok_rows, heads_here * VALUE_SIZE)
        .astype(jnp.bfloat16)
    )
    head_sum = summed_on_arrival(
        jnp.dot(attended, out_weight, preferred_element_type=jnp.float32).astype(jnp.bfloat16),
        "tp",
        0,
    )
    mixed_own = (
        lax.dynamic_slice_in_dim(residual, tp_index * own_rows, own_rows, 0).astype(jnp.float32)
        + head_sum
    )
    normed_own = norm_rows(mixed_own, ffn_gain).astype(jnp.bfloat16)
    normed_all = collect(normed_own, "tp", 0)
    gate = jnp.dot(normed_all, gate_full, preferred_element_type=jnp.float32)
    up_part = jnp.dot(normed_all, up_full, preferred_element_type=jnp.float32)
    hidden = (jax.nn.silu(gate) * up_part).astype(jnp.bfloat16)
    terms = jnp.dot(
        hidden,
        lax.all_gather(down_weight, "sp", axis=1, tiled=True),
        preferred_element_type=jnp.float32,
    )
    ffn_own = summed_on_arrival(terms.astype(jnp.bfloat16), "tp", 0)
    return (mixed_own + ffn_own).astype(jnp.bfloat16)


def solution(mesh):
    return jax.shard_map(
        local,
        mesh=mesh,
        in_specs=(
            P(("grp", "sp"), "tp"),
            P(("grp", "sp"), "tp"),
            P(("grp", "sp"), None),
            P(("grp", "sp"), None),
            P(),
            P(),
            P(),
            P(("grp", "sp"), None),
            P("tp", None),
            P(),
            P("sp", "tp"),
            P("sp", "tp"),
            P("tp", "sp"),
        ),
        out_specs=P(("grp", "sp", "tp"), None),
        check_vma=False,
    )
```

profile of v0, /device:TPU:40, one launch (start us, length us, event | category | flops | bytes accessed | tf_op | source)
XLA Modules:
  0.0 341.1 jit_solution(13385910839321723179)
XLA Ops:
  15.8 52.6 %all-gather = bf16[32,320,32]{1,2,0:T(8,128)(2,1)S(1)} all-gather(bf16[1,320,32]{1,2,0:T(8,128)(2,1)S(1)} %bitcast.89), channel_id=1, replica_groups=mesh['grp'=2,'sp'=32,'tp'=4] {'sp'}, dimensions={0}, use_global_device_ids=true | all-gather | bytes 675840 | tf_op jit(solution)/shard_map/all_gather | solution.py:141
  72.4 24.7 %all-gather.5.cloned.1.call-done = bf16[10240,256]{1,0:T(8,128)(2,1)} async-done(((bf16[320,256]{1,0:T(8,128)(2,1)}), bf16[10240,256]{1,0:T(8,128)(2,1)}) %all-gather.5.cloned.1.call-update) | async-done | bytes 5242896 | tf_op jit(solution)/shard_map/all_gather | solution.py:140
  97.1 152.5 %while.15 = (s32[]{:T(128)}, f32[4,320]{1,0:T(4,128)S(1)}, f32[4,320]{1,0:T(4,128)S(1)}, f32[320,4,64]{0,2,1:T(8,128)S(1)}, bf16[16,640,256]{2,1,0:T(8,128)(2,1)...) while((s32[]{:T(128)}, f32[4,320]{1,0:T(4,128)S(1)}, ...), condition=%wide.region_4.5_spmd.clone, body=%wide.region_1.4_spmd.clone.sunk | while | flops 436231680 | bytes 32760992 | solution.py:155
  102.9 2.7 fusion.90
  108.5 2.4 fusion.86
  112.4 2.7 fusion.90
  118.0 2.4 fusion.86
  121.9 2.8 fusion.90
  127.5 2.4 fusion.86
  131.4 2.7 fusion.90
  140.9 2.8 fusion.90
  146.6 2.4 fusion.86
  150.5 2.8 fusion.90
  160.1 2.8 fusion.90
  169.6 2.8 fusion.90
  179.2 2.7 fusion.90
  188.7 2.9 fusion.90
  198.3 2.8 fusion.90
  203.9 2.4 fusion.86
  207.8 2.7 fusion.90
  217.3 2.8 fusion.90
  223.0 2.4 fusion.86
  226.8 2.8 fusion.90
  236.4 2.7 fusion.90
  242.0 2.4 fusion.86
  245.9 2.8 fusion.90
  251.2 4.2 %all-to-all-start = ((bf16[4,80,2048]{2,1,0:T(8,128)(2,1)}), bf16[4,80,2048]{2,1,0:T(8,128)(2,1)S(1)}, u32[]{:S(2)}, u32[]{:S(2)}) async-start(bf16[4,80,2048]{2,1,0:T(8,128)(2,1)} %bitcast.80), calls=%async_computation | async-start | bytes 2621440 | tf_op jit(solution)/shard_map/all_to_all | solution.py:27
  255.4 18.3 %all-to-all-done = bf16[4,80,2048]{2,1,0:T(8,128)(2,1)S(1)} async-done(((bf16[4,80,2048]{2,1,0:T(8,128)(2,1)}), bf16[4,80,2048]{2,1,0:T(8,128)(2,1)S(1)}, u32[]{:S(2)}, u32[]{:S(2)}) %all-to-all-start) | async-done | bytes 1310752 | tf_op jit(solution)/shard_map/all_to_all | solution.py:27
  276.4 20.0 %all_to_all.15 = bf16[4,80,2048]{2,1,0:T(8,128)(2,1)S(1)} all-to-all(bf16[4,80,2048]{2,1,0:T(8,128)(2,1)S(1)} %broadcast_in_dim.11), channel_id=1, replica_groups=mesh['grp'=2,'sp'=32,'tp'=4] {'tp'}, dimensions={0} | all-to-all | bytes 2621440 | tf_op jit(solution)/shard_map/all_to_all | solution.py:33
  296.4 6.1 %fusion.25 = f32[320,1408]{1,0:T(8,128)} fusion(bf16[320,2048]{1,0:T(8,128)(2,1)S(1)} %bitcast.83, bf16[2048,2816]{1,0:T(8,128)(2,1)} %all-gather.7.cloned.1.call-done), kind=kOutput, calls=%fused_computation.28 | convolution fusion | flops 1845493760 | bytes 8880128 | tf_op jit(solution)/shard_map/dot_general | solution.py:173
  302.5 10.2 %convolution_convert_fusion.2 = bf16[320,2048]{1,0:T(8,128)(2,1)} fusion(bf16[1408,2048]{0,1:T(8,128)(2,1)} %all-gather.9.cloned.1.call-done, bf16[320,2048]{1,0:T(8,128)(2,1)S(1)} %bitcast.84, bf16[2048,2816]{1,0:T(8,128)(2,1)} %all-gather.7.cloned.1.call-done, f32[320,1408]{1,0:T(8,128)} %fusion.25), kind=kOutput, calls=%fused_computation.31 | convolution fusion | flops 3694346240 | bytes 15958016 | tf_op jit(solution)/shard_map/dot_general | solution.py:176
  312.6 19.9 %all_to_all.16 = bf16[4,80,2048]{2,1,0:T(8,128)(2,1)S(1)} all-to-all(bf16[4,80,2048]{2,1,0:T(8,128)(2,1)} %bitcast.85), channel_id=1, replica_groups=mesh['grp'=2,'sp'=32,'tp'=4] {'tp'}, dimensions={0} | all-to-all | bytes 2621440 | tf_op jit(solution)/shard_map/all_to_all | solution.py:27
  (197 shorter events, 109.4 us)
Async XLA Ops:
  6.5 243.1 %copy-start = (bf16[256,2048]{1,0:T(8,128)(2,1)S(1)}, bf16[256,2048]{1,0:T(8,128)(2,1)}, u32[]{:S(2)}) copy-start(bf16[256,2048]{1,0:T(8,128)(2,1)} %param.23) | copy-start | bytes 3145732
  6.6 90.5 %all-gather.5.cloned.1.call-start = ((), (), s32[]{:S(2)}) async-start(), calls=%async_computation.3 | async-start | bytes 5406720 | tf_op jit(solution)/shard_map/all_gather | solution.py:140
  9.5 286.9 %all-gather.7.cloned.1.call-start = ((), (), s32[]{:S(2)}) async-start(), calls=%async_computation.4 | async-start | bytes 11894784 | tf_op jit(solution)/shard_map/all_gather | solution.py:15
  11.4 291.0 %all-gather.9.cloned.1.call-start = ((), (), s32[]{:S(2)}) async-start(), calls=%async_computation.5 | async-start | bytes 5947392 | tf_op jit(solution)/shard_map/all_gather | solution.py:178
  101.4 4.2 %copy-start.1 = (f32[4,320,640]{2,1,0:T(8,128)S(1)}, f32[4,320,640]{2,1,0:T(8,128)}, u32[]{:S(2)}) copy-start(f32[4,320,640]{2,1,0:T(8,128)} %get-tuple-element.224) | copy-start | bytes 9830404 | tf_op jit(solution)/shard_map/while
  110.9 4.2 %copy-start.1 = (f32[4,320,640]{2,1,0:T(8,128)S(1)}, f32[4,320,640]{2,1,0:T(8,128)}, u32[]{:S(2)}) copy-start(f32[4,320,640]{2,1,0:T(8,128)} %get-tuple-element.224) | copy-start | bytes 9830404 | tf_op jit(solution)/shard_map/while
  120.4 4.3 %copy-start.1 = (f32[4,320,640]{2,1,0:T(8,128)S(1)}, f32[4,320,640]{2,1,0:T(8,128)}, u32[]{:S(2)}) copy-start(f32[4,320,640]{2,1,0:T(8,128)} %get-tuple-element.224) | copy-start | bytes 9830404 | tf_op jit(solution)/shard_map/while
  130.0 4.2 %copy-start.1 = (f32[4,320,640]{2,1,0:T(8,128)S(1)}, f32[4,320,640]{2,1,0:T(8,128)}, u32[]{:S(2)}) copy-start(f32[4,320,640]{2,1,0:T(8,128)} %get-tuple-element.224) | copy-start | bytes 9830404 | tf_op jit(solution)/shard_map/while
  139.5 4.3 %copy-start.1 = (f32[4,320,640]{2,1,0:T(8,128)S(1)}, f32[4,320,640]{2,1,0:T(8,128)}, u32[]{:S(2)}) copy-start(f32[4,320,640]{2,1,0:T(8,128)} %get-tuple-element.224) | copy-start | bytes 9830404 | tf_op jit(solution)/shard_map/while
  149.0 4.3 %copy-start.1 = (f32[4,320,640]{2,1,0:T(8,128)S(1)}, f32[4,320,640]{2,1,0:T(8,128)}, u32[]{:S(2)}) copy-start(f32[4,320,640]{2,1,0:T(8,128)} %get-tuple-element.224) | copy-start | bytes 9830404 | tf_op jit(solution)/shard_map/while
  158.6 4.3 %copy-start.1 = (f32[4,320,640]{2,1,0:T(8,128)S(1)}, f32[4,320,640]{2,1,0:T(8,128)}, u32[]{:S(2)}) copy-start(f32[4,320,640]{2,1,0:T(8,128)} %get-tuple-element.224) | copy-start | bytes 9830404 | tf_op jit(solution)/shard_map/while
  168.2 4.3 %copy-start.1 = (f32[4,320,640]{2,1,0:T(8,128)S(1)}, f32[4,320,640]{2,1,0:T(8,128)}, u32[]{:S(2)}) copy-start(f32[4,320,640]{2,1,0:T(8,128)} %get-tuple-element.224) | copy-start | bytes 9830404 | tf_op jit(solution)/shard_map/while
  177.7 4.2 %copy-start.1 = (f32[4,320,640]{2,1,0:T(8,128)S(1)}, f32[4,320,640]{2,1,0:T(8,128)}, u32[]{:S(2)}) copy-start(f32[4,320,640]{2,1,0:T(8,128)} %get-tuple-element.224) | copy-start | bytes 9830404 | tf_op jit(solution)/shard_map/while
  187.2 4.3 %copy-start.1 = (f32[4,320,640]{2,1,0:T(8,128)S(1)}, f32[4,320,640]{2,1,0:T(8,128)}, u32[]{:S(2)}) copy-start(f32[4,320,640]{2,1,0:T(8,128)} %get-tuple-element.224) | copy-start | bytes 9830404 | tf_op jit(solution)/shard_map/while
  196.8 4.2 %copy-start.1 = (f32[4,320,640]{2,1,0:T(8,128)S(1)}, f32[4,320,640]{2,1,0:T(8,128)}, u32[]{:S(2)}) copy-start(f32[4,320,640]{2,1,0:T(8,128)} %get-tuple-element.224) | copy-start | bytes 9830404 | tf_op jit(solution)/shard_map/while
  206.4 4.2 %copy-start.1 = (f32[4,320,640]{2,1,0:T(8,128)S(1)}, f32[4,320,640]{2,1,0:T(8,128)}, u32[]{:S(2)}) copy-start(f32[4,320,640]{2,1,0:T(8,128)} %get-tuple-element.224) | copy-start | bytes 9830404 | tf_op jit(solution)/shard_map/while
  215.9 4.2 %copy-start.1 = (f32[4,320,640]{2,1,0:T(8,128)S(1)}, f32[4,320,640]{2,1,0:T(8,128)}, u32[]{:S(2)}) copy-start(f32[4,320,640]{2,1,0:T(8,128)} %get-tuple-element.224) | copy-start | bytes 9830404 | tf_op jit(solution)/shard_map/while
  225.4 4.2 %copy-start.1 = (f32[4,320,640]{2,1,0:T(8,128)S(1)}, f32[4,320,640]{2,1,0:T(8,128)}, u32[]{:S(2)}) copy-start(f32[4,320,640]{2,1,0:T(8,128)} %get-tuple-element.224) | copy-start | bytes 9830404 | tf_op jit(solution)/shard_map/while
  234.9 4.2 %copy-start.1 = (f32[4,320,640]{2,1,0:T(8,128)S(1)}, f32[4,320,640]{2,1,0:T(8,128)}, u32[]{:S(2)}) copy-start(f32[4,320,640]{2,1,0:T(8,128)} %get-tuple-element.224) | copy-start | bytes 9830404 | tf_op jit(solution)/shard_map/while
  244.4 4.2 %copy-start.1 = (f32[4,320,640]{2,1,0:T(8,128)S(1)}, f32[4,320,640]{2,1,0:T(8,128)}, u32[]{:S(2)}) copy-start(f32[4,320,640]{2,1,0:T(8,128)} %get-tuple-element.224) | copy-start | bytes 9830404 | tf_op jit(solution)/shard_map/while
  251.2 23.9 %copy-start.2 = (f32[2048]{0:T(1024)S(1)}, f32[2048]{0:T(1024)}, u32[]{:S(2)}) copy-start(f32[2048]{0:T(1024)} %param.24) | copy-start | bytes 24580
  251.2 22.5 %all-to-all-start = ((bf16[4,80,2048]{2,1,0:T(8,128)(2,1)}), bf16[4,80,2048]{2,1,0:T(8,128)(2,1)S(1)}, u32[]{:S(2)}, u32[]{:S(2)}) async-start(bf16[4,80,2048]{2,1,0:T(8,128)(2,1)} %bitcast.80), calls=%async_computation | async-start | bytes 2621440 | tf_op jit(solution)/shard_map/all_to_all | solution.py:27
Sparse Core Ops, SparseCore 0:
  9.6 87.3 all-gather.4
  98.9 77.7 all-gather.6
  178.5 70.0 all-gather.8
where the time goes:
time: 343 us; the launch traced here: 341 us
  matrix products  155 us (45%)
  blocking collectives  92.5 us (27%)
  waiting for transfers between devices  43.8 us (13%)
  other arithmetic  27.3 us (8%)
  between operations  13.3 us (4%)
  starting transfers between devices  4.32 us (1%)
  local copies, waits for them, and re-layouts  4.2 us (1%)
    all_gather x1, blocking collectives, local(): rope_piece = lax.all_gather(key_turned, 'sp', axis=0, tiled=True)  52.6 us
    dot_general x16, matrix products, absorb(): jnp.einsum('hqk,khd->qhd', weights.astype(jnp.bfloat16), value_rows, pref...  44.4 us
    dot_general x16, matrix products, absorb(): jnp.einsum('qhd,kd->hqk', query_turned, rope_block, preferred_element_typ...  39 us
    all_gather x1, waiting for transfers between devices, local(): latent_piece = lax.all_gather(latent, 'sp', axis=0, tiled=True)  24.7 us
    dot_general x16, matrix products, absorb(): jnp.dot(latent_block, value_cols, preferred_element_type=jnp.float32)  22.9 us
    dot_general x16, matrix products, absorb(): jnp.dot(latent_block, key_cols, preferred_element_type=jnp.float32)  20.4 us
    all_to_all x1, blocking collectives, sent_to_all(): return lax.all_to_all(copies, axis, split_axis=0, concat_axis=0, tiled=True)  20 us
    all_to_all x1, blocking collectives, summed_on_arrival(): parts = lax.all_to_all(cut_along(array, dim, count), axis, 0, 0, tiled=True)  19.9 us
  transfers between devices with their start and end apart: 4, of which 2 were waited for; matrix products, arithmetic and copies ran while one was open for 50% of the time, Pallas kernels for 0%

commit v1 on v0

--- a/solution.py
+++ b/solution.py
@@ -137,7 +137,9 @@
         jnp.zeros((tok_rows, heads_here, VALUE_SIZE), jnp.float32),
     )
     carried = initial
-    latent_piece = lax.all_gather(latent, "sp", axis=0, tiled=True)
+    latent_piece = jnp.concatenate(
+        lax.all_to_all(jnp.stack([latent] * lax.axis_size("sp")), "sp", 0, 0), axis=0
+    )
     rope_piece = lax.all_gather(key_turned, "sp", axis=0, tiled=True)
     shard_count = latent_piece.shape[0] // tok_rows
     grouped = max(

time: 343 us -> 600 us (1.75)
  blocking collectives: 92.5 us -> 348 us
  starting transfers between devices: 4.32 us -> 29.5 us
  waiting for transfers between devices: 43.8 us -> 19.1 us
    all_gather x1, blocking collectives: 52.6 us -> 308 us  [local(): rope_piece = lax.all_gather(key_turned, 'sp', axis=0, tiled=True)]
    all_to_all x0 -> x1, starting transfers between devices: none -> 24.9 us  [local(): lax.all_to_all(jnp.stack([latent] * lax.axis_size('sp')), 'sp', 0, 0)]
    all_gather x1 -> x0, waiting for transfers between devices: 24.7 us -> none  [local(): latent_piece = lax.all_gather(latent, 'sp', axis=0, tiled=True)]
  transfers between devices with their start and end apart: 4 -> 4, of which waited for: 2 -> 1; matrix products, arithmetic and copies ran while one was open for 50% -> 29% of each run, Pallas kernels for 0% -> 0%
where the time goes in v1:
time: 600 us; the launch traced here: 598 us
  blocking collectives  348 us (58%)
  matrix products  154 us (26%)
  starting transfers between devices  29.5 us (5%)
  other arithmetic  25.9 us (4%)
  waiting for transfers between devices  19.1 us (3%)
  between operations  13.7 us (2%)
  local copies, waits for them, and re-layouts  6.67 us (1%)
    all_gather x1, blocking collectives, local(): rope_piece = lax.all_gather(key_turned, 'sp', axis=0, tiled=True)  308 us
    dot_general x16, matrix products, absorb(): jnp.einsum('hqk,khd->qhd', weights.astype(jnp.bfloat16), value_rows, pref...  43.9 us
    dot_general x16, matrix products, absorb(): jnp.einsum('qhd,kd->hqk', query_turned, rope_block, preferred_element_typ...  39.1 us
    all_to_all x1, starting transfers between devices, local(): lax.all_to_all(jnp.stack([latent] * lax.axis_size('sp')), 'sp', 0, 0)  24.9 us
    dot_general x16, matrix products, absorb(): jnp.dot(latent_block, value_cols, preferred_element_type=jnp.float32)  22.8 us
    dot_general x16, matrix products, absorb(): jnp.dot(latent_block, key_cols, preferred_element_type=jnp.float32)  20.4 us
    all_to_all x1, blocking collectives, sent_to_all(): return lax.all_to_all(copies, axis, split_axis=0, concat_axis=0, tiled=True)  19.9 us
    all_to_all x1, blocking collectives, summed_on_arrival(): parts = lax.all_to_all(cut_along(array, dim, count), axis, 0, 0, tiled=True)  19.9 us
  transfers between devices with their start and end apart: 4, of which 1 were waited for; matrix products, arithmetic and copies ran while one was open for 29% of the time, Pallas kernels for 0%

profile of v1, /device:TPU:40, one launch (start us, length us, event | category | flops | bytes accessed | tf_op | source)
XLA Modules:
  0.0 597.8 jit_solution(10977336075720100528)
XLA Ops:
  10.6 3.0 stack.10
  13.6 24.9 %all-to-all-start = ((bf16[32,320,256]{2,1,0:T(8,128)(2,1)}), bf16[32,320,256]{2,1,0:T(8,128)(2,1)}, u32[]{:S(2)}, u32[]{:S(2)}) async-start(bf16[32,320,256]{2,1,0:T(8,128)(2,1)} %stack.10), calls=%async_computation | async-start | bytes 10485760 | tf_op jit(solution)/shard_map/all_to_all | solution.py:141
  40.8 308.0 %all-gather = bf16[32,320,32]{1,2,0:T(8,128)(2,1)S(1)} all-gather(bf16[1,320,32]{1,2,0:T(8,128)(2,1)S(1)} %bitcast.88), channel_id=1, replica_groups=mesh['grp'=2,'sp'=32,'tp'=4] {'sp'}, dimensions={0}, use_global_device_ids=true | all-gather | bytes 675840 | tf_op jit(solution)/shard_map/all_gather | solution.py:143
  353.7 152.0 %while.15 = (s32[]{:T(128)}, f32[4,320]{1,0:T(4,128)S(1)}, f32[4,320]{1,0:T(4,128)S(1)}, f32[320,4,64]{0,2,1:T(8,128)S(1)}, bf16[16,640,256]{2,1,0:T(8,128)(2,1)...) while((s32[]{:T(128)}, f32[4,320]{1,0:T(4,128)S(1)}, ...), condition=%wide.region_4.5_spmd.clone, body=%wide.region_1.4_spmd.clone.sunk | while | flops 436231680 | bytes 32760992 | solution.py:157
  359.5 2.7 fusion.90
  365.1 2.4 fusion.86
  369.0 2.8 fusion.90
  378.6 2.7 fusion.90
  388.1 2.8 fusion.90
  397.6 2.8 fusion.90
  403.2 2.4 fusion.86
  407.1 2.7 fusion.90
  416.6 2.7 fusion.90
  422.2 2.4 fusion.86
  426.1 2.7 fusion.90
  435.6 2.7 fusion.90
  441.2 2.4 fusion.86
  445.1 2.7 fusion.90
  454.6 2.7 fusion.90
  460.2 2.4 fusion.86
  464.1 2.7 fusion.90
  473.6 2.7 fusion.90
  479.2 2.4 fusion.86
  483.1 2.7 fusion.90
  492.6 2.7 fusion.90
  502.1 2.7 fusion.90
  507.4 4.5 all-to-all-start.1
  511.9 18.3 %all-to-all-done.1 = bf16[4,80,2048]{2,1,0:T(8,128)(2,1)S(1)} async-done(((bf16[4,80,2048]{2,1,0:T(8,128)(2,1)}), bf16[4,80,2048]{2,1,0:T(8,128)(2,1)S(1)}, u32[]{:S(2)}, u32[]{:S(2)}) %all-to-all-start.1) | async-done | bytes 1310752 | tf_op jit(solution)/shard_map/all_to_all | solution.py:27
  532.9 19.9 %all_to_all.20 = bf16[4,80,2048]{2,1,0:T(8,128)(2,1)S(1)} all-to-all(bf16[4,80,2048]{2,1,0:T(8,128)(2,1)S(1)} %broadcast_in_dim.11), channel_id=1, replica_groups=mesh['grp'=2,'sp'=32,'tp'=4] {'tp'}, dimensions={0} | all-to-all | bytes 2621440 | tf_op jit(solution)/shard_map/all_to_all | solution.py:33
  552.8 6.1 %fusion.25 = f32[320,1408]{1,0:T(8,128)} fusion(bf16[320,2048]{1,0:T(8,128)(2,1)S(1)} %bitcast.82, bf16[2048,2816]{1,0:T(8,128)(2,1)} %all-gather.4.cloned.1.call-done), kind=kOutput, calls=%fused_computation.28 | convolution fusion | flops 1845493760 | bytes 8880128 | tf_op jit(solution)/shard_map/dot_general | solution.py:175
  558.9 10.2 %convolution_convert_fusion.2 = bf16[320,2048]{1,0:T(8,128)(2,1)} fusion(bf16[1408,2048]{0,1:T(8,128)(2,1)} %all-gather.6.cloned.1.call-done, bf16[320,2048]{1,0:T(8,128)(2,1)S(1)} %bitcast.83, bf16[2048,2816]{1,0:T(8,128)(2,1)} %all-gather.4.cloned.1.call-done, f32[320,1408]{1,0:T(8,128)} %fusion.25), kind=kOutput, calls=%fused_computation.31 | convolution fusion | flops 3694346240 | bytes 15958016 | tf_op jit(solution)/shard_map/dot_general | solution.py:178
  569.1 19.9 %all_to_all.21 = bf16[4,80,2048]{2,1,0:T(8,128)(2,1)S(1)} all-to-all(bf16[4,80,2048]{2,1,0:T(8,128)(2,1)} %bitcast.84), channel_id=1, replica_groups=mesh['grp'=2,'sp'=32,'tp'=4] {'tp'}, dimensions={0} | all-to-all | bytes 2621440 | tf_op jit(solution)/shard_map/all_to_all | solution.py:27
  (205 shorter events, 109.9 us)
Async XLA Ops:
  6.5 499.2 %copy-start = (bf16[256,2048]{1,0:T(8,128)(2,1)S(1)}, bf16[256,2048]{1,0:T(8,128)(2,1)}, u32[]{:S(2)}) copy-start(bf16[256,2048]{1,0:T(8,128)(2,1)} %param.23) | copy-start | bytes 3145732
  6.6 546.3 %all-gather.4.cloned.1.call-start = ((), (), s32[]{:S(2)}) async-start(), calls=%async_computation.4 | async-start | bytes 11894784 | tf_op jit(solution)/shard_map/all_gather | solution.py:15
  13.6 25.8 %copy-start.2 = (bf16[320,128]{1,0:T(8,128)(2,1)S(1)}, bf16[320,128]{1,0:T(8,128)(2,1)}, u32[]{:S(2)}) copy-start(bf16[320,128]{1,0:T(8,128)(2,1)} %param.16) | copy-start | bytes 245764
  13.6 26.6 %copy-start.4 = (bf16[320,32]{0,1:T(8,128)(2,1)S(1)}, bf16[320,32]{0,1:T(8,128)(2,1)}, u32[]{:S(2)}) copy-start(bf16[320,32]{0,1:T(8,128)(2,1)} %param.18) | copy-start | bytes 61444
  13.6 340.1 %all-to-all-start = ((bf16[32,320,256]{2,1,0:T(8,128)(2,1)}), bf16[32,320,256]{2,1,0:T(8,128)(2,1)}, u32[]{:S(2)}, u32[]{:S(2)}) async-start(bf16[32,320,256]{2,1,0:T(8,128)(2,1)} %stack.10), calls=%async_computation | async-start | bytes 10485760 | tf_op jit(solution)/shard_map/all_to_all | solution.py:141
  38.5 520.4 %all-gather.6.cloned.1.call-start = ((), (), s32[]{:S(2)}) async-start(), calls=%async_computation.5 | async-start | bytes 5947392 | tf_op jit(solution)/shard_map/all_gather | solution.py:180
  40.2 0.6 copy-start.6
  40.3 0.6 copy-start.3
  358.1 4.2 copy-start.1
  367.6 4.2 copy-start.1
  377.1 4.2 copy-start.1
  386.6 4.2 copy-start.1
  396.2 4.2 copy-start.1
  405.7 4.2 copy-start.1
  415.2 4.2 copy-start.1
  424.7 4.2 copy-start.1
  434.2 4.2 copy-start.1
  443.7 4.2 copy-start.1
  453.1 4.2 copy-start.1
  462.6 4.2 copy-start.1
  472.1 4.2 copy-start.1
  481.6 4.2 copy-start.1
  491.1 4.2 copy-start.1
  500.6 4.2 copy-start.1
  507.4 24.2 %copy-start.5 = (f32[2048]{0:T(1024)S(1)}, f32[2048]{0:T(1024)}, u32[]{:S(2)}) copy-start(f32[2048]{0:T(1024)} %param.24) | copy-start | bytes 24580
  507.4 22.8 %all-to-all-start.1 = ((bf16[4,80,2048]{2,1,0:T(8,128)(2,1)}), bf16[4,80,2048]{2,1,0:T(8,128)(2,1)S(1)}, u32[]{:S(2)}, u32[]{:S(2)}) async-start(bf16[4,80,2048]{2,1,0:T(8,128)(2,1)} %bitcast.80), calls=%async_computation.1 | async-start | bytes 2621440 | tf_op jit(solution)/shard_map/all_to_all | solution.py:27
Sparse Core Ops, SparseCore 0:
  9.2 315.3 all-gather.3
  326.4 73.2 all-gather.5
